TPU v7x, 32 devices: a whole 2x2x4 slice. The times are simulated.
32 devices in a mesh: grp: 2 (over y), sp: 4 (over z), tp: 4 (over x, core).
Axes of the slice: x: 2, y: 2, z: 4, core: 2. Of those that a mesh axis runs over, the one named last changes fastest.
Arguments:
- residual: bfloat16 [2048, 2048], P(('grp', 'sp', 'tp')), parts along dimension 0, may hold values from -6 to 6
- query_nope: bfloat16 [2048, 1024], P(('grp', 'sp'), 'tp'), parts along dimension 0, may hold values from -6 to 6
- query_rope: bfloat16 [2048, 512], P(('grp', 'sp'), 'tp'), parts along dimension 0, may hold values from -240 to 240
- kv_latent: bfloat16 [2048, 256], P(('grp', 'sp')), parts along dimension 0, may hold values from -6 to 6
- rope_key: bfloat16 [2048, 64], P(('grp', 'sp')), parts along dimension 0, may hold values from -6 to 6
- latent_gain: float32 [256], replicated, may hold values from 0.1 to 1.9
- w_key: bfloat16 [256, 1024], P(None, 'tp'), may hold values from -0.375 to 0.375
- w_value: bfloat16 [256, 1024], P(None, 'tp'), may hold values from -0.375 to 0.375
- w_out: bfloat16 [1024, 2048], P('tp'), may hold values from -0.1875 to 0.1875
- post_gain: float32 [2048], replicated, may hold values from 0.1 to 1.9
- routes: int32 [2048, 2], P(('grp', 'sp', 'tp')), parts along dimension 0, may hold values from 0 to 3, all different within a row; in each aligned block of 64 rows (0 to 63, 64 to 127, ...) at most 48 rows name the same one
- route_weight: float32 [2048, 2], P(('grp', 'sp', 'tp')), parts along dimension 0, may hold values from 0.25 to 1
- moe_gain: float32 [2048], replicated, may hold values from 0.1 to 1.9
- w_gate: bfloat16 [4, 2048, 3584], P('sp', None, 'tp'), may hold values from -0.125 to 0.125
- w_up: bfloat16 [4, 2048, 3584], P('sp', None, 'tp'), may hold values from -0.125 to 0.125
- w_down: bfloat16 [4, 3584, 2048], P('sp', 'tp'), may hold values from -0.09375 to 0.09375
Outputs:
- mixed: bfloat16 [2048, 2048], P(('grp', 'sp', 'tp')), parts along dimension 0
There are 2 independent parts, one for each index of `grp`. A program takes and returns all parts, laid end to end along the dimension named above; an argument that names none is the same for every part. Nothing has to cross between parts.
Inputs may be any that keep to these rules, and one draw needn't show every extreme that they name: `routes`: each row names two different experts. Among the 64 rows of one device no expert is named more than 48 times, and some device names some expert exactly 48 times.
All inputs are finite; a program needn't handle non-finite values.
Results may differ from a plain program's by a relative error of at most 0.014.
Values may be sent and summed in bfloat16 or wider, within the bound.
A program may use at most 128 MiB of HBM per device.

v0:
```python
import jax
import jax.numpy as jnp
from jax import lax
from jax.sharding import PartitionSpec as P

HEADS = 8
NOPE = 128
ROPE = 64
VDIM = 128
epsilon = 1e-06
rope_base = 10000.0


def rms_scale(inputs, gain_vector):
    mean_square = jnp.mean(inputs * inputs, axis=-1, keepdims=True)
    return inputs * lax.rsqrt(mean_square + epsilon) * gain_vector


def tables(positions, rot_width):
    frequency = 1.0 / rope_base ** (jnp.arange(0, rot_width, 2, dtype=jnp.float32) / rot_width)
    angles = positions.astype(jnp.float32)[:, None] * frequency[None, :]
    return (jnp.cos(angles), jnp.sin(angles))


def rotate(inputs, cosine_table, sine_table):
    half_width = inputs.shape[-1] // 2
    first_half = inputs[..., :half_width]
    second_half = inputs[..., half_width:]
    return jnp.concatenate(
        [
            first_half * cosine_table - second_half * sine_table,
            second_half * cosine_table + first_half * sine_table,
        ],
        axis=-1,
    )


def expand(latent_rows, rope_rows, latent_gain, w_key, w_value):
    normed = rms_scale(latent_rows.astype(jnp.float32), latent_gain).astype(jnp.bfloat16)
    key_plain = jnp.dot(normed, w_key, preferred_element_type=jnp.float32).astype(jnp.bfloat16)
    value_plain = jnp.dot(normed, w_value, preferred_element_type=jnp.float32).astype(jnp.bfloat16)
    key_positions = jnp.arange(latent_rows.shape[0], dtype=jnp.int32)
    cosine_table, sine_table = tables(key_positions, rope_rows.shape[1])
    key_turned = rotate(rope_rows.astype(jnp.float32), cosine_table, sine_table).astype(
        jnp.bfloat16
    )
    return (key_plain, value_plain, key_turned)


def body(
    residual,
    query_nope,
    query_rope,
    kv_latent,
    rope_key,
    latent_gain,
    w_key,
    w_value,
    w_out,
    post_gain,
    routes,
    route_weight,
    moe_gain,
    w_gate,
    w_up,
    w_down,
):
    tok_rows = query_nope.shape[0]
    heads_here = HEADS // lax.axis_size("tp")
    first_row = lax.axis_index("sp") * tok_rows
    last_row = first_row + tok_rows - 1
    positions = first_row + jnp.arange(tok_rows, dtype=jnp.int32)
    cosine_table, sine_table = tables(positions, ROPE)
    query_plain = query_nope.reshape(tok_rows, heads_here, NOPE)
    query_turned = rotate(
        query_rope.reshape(tok_rows, heads_here, ROPE).astype(jnp.float32),
        cosine_table[:, None, :],
        sine_table[:, None, :],
    ).astype(jnp.bfloat16)
    score_scale = (NOPE + ROPE) ** (-0.5)

    def update(state_now, key_plain, value_plain, key_turned):
        row_max, row_sum, running = state_now
        key_count = key_plain.shape[0]
        key_heads = key_plain.reshape(key_count, heads_here, NOPE)
        value_heads = value_plain.reshape(key_count, heads_here, VDIM)
        scores = jnp.einsum(
            "thd,shd->hts", query_plain, key_heads, preferred_element_type=jnp.float32
        )
        scores = (
            scores
            + jnp.einsum(
                "thd,sd->hts", query_turned, key_turned, preferred_element_type=jnp.float32
            )
        ) * score_scale
        key_positions = jnp.arange(key_count, dtype=jnp.int32)
        allowed = key_positions[None, :] <= positions[:, None]
        scores = jnp.where(allowed[None], scores, -1e30)
        new_max = jnp.maximum(row_max, jnp.max(scores, axis=-1))
        weights = jnp.exp(scores - new_max[..., None])
        row_sum = jnp.sum(weights, axis=-1)
        running = jnp.einsum(
            "hts,shd->htd",
            weights.astype(jnp.bfloat16),
            value_heads,
            preferred_element_type=jnp.float32,
        )
        return (new_max, row_sum, running)

    start_state = (
        jnp.full((heads_here, tok_rows), -1e30, jnp.float32),
        jnp.zeros((heads_here, tok_rows), jnp.float32),
        jnp.zeros((heads_here, tok_rows, VDIM), jnp.float32),
    )
    pieces = (
        lax.all_gather(kv_latent, "sp", axis=0, tiled=True),
        lax.all_gather(rope_key, "sp", axis=0, tiled=True),
    )

    def take_piece(state_in):
        key_plain, value_plain, key_turned = expand(
            pieces[0], pieces[1], latent_gain, w_key, w_value
        )
        return update(state_in, key_plain, value_plain, key_turned)

    def skip_piece(state_in):
        return state_in

    final_state = lax.cond(jnp.int32(0) <= last_row, take_piece, skip_piece, start_state)
    attended = (final_state[2] / final_state[1][..., None]).transpose(1, 0, 2)
    attended = attended.reshape(tok_rows, heads_here * VDIM).astype(jnp.bfloat16)
    chosen = attended
    product = jnp.dot(chosen, w_out, preferred_element_type=jnp.float32)
    branch = lax.psum_scatter(
        product.astype(jnp.bfloat16).astype(jnp.float32).astype(jnp.bfloat16),
        "tp",
        scatter_dimension=0,
        tiled=True,
    ).astype(jnp.float32)
    updated = (residual.astype(jnp.float32) + rms_scale(branch, post_gain)).astype(jnp.bfloat16)
    moe_in = rms_scale(updated.astype(jnp.float32), moe_gain).astype(jnp.bfloat16)
    token_count = routes.shape[0]
    experts = lax.axis_size("sp")
    capacity = max(2, 3 * token_count // experts)
    onehot = (routes[:, :, None] == jnp.arange(experts, dtype=jnp.int32)[None, None, :]).astype(
        jnp.int32
    )
    flat_hits = onehot.reshape(token_count * 2, experts)
    order_in = jnp.cumsum(flat_hits, axis=0) - flat_hits
    slot_ids = jnp.sum(
        (order_in + jnp.arange(experts, dtype=jnp.int32)[None, :] * capacity) * flat_hits, axis=1
    )
    placing = slot_ids[:, None] == jnp.arange(experts * capacity, dtype=jnp.int32)[None, :]
    placing = placing.astype(jnp.bfloat16).reshape(token_count, 2, experts * capacity)
    sending = jnp.einsum("tks,td->sd", placing, moe_in, preferred_element_type=jnp.float32).astype(
        jnp.bfloat16
    )
    received = lax.all_to_all(sending, "sp", split_axis=0, concat_axis=0, tiled=True)
    span_rows = lax.all_gather(received, "tp", axis=0, tiled=True)
    gate_pre = jnp.dot(span_rows, w_gate[0], preferred_element_type=jnp.float32)
    up_proj = jnp.dot(span_rows, w_up[0], preferred_element_type=jnp.float32)
    hidden_rows = (jax.nn.silu(gate_pre) * up_proj).astype(jnp.bfloat16)
    chosen = hidden_rows
    product = jnp.dot(chosen, w_down[0], preferred_element_type=jnp.float32)
    expert_out = lax.psum_scatter(
        product.astype(jnp.bfloat16).astype(jnp.float32).astype(jnp.bfloat16),
        "tp",
        scatter_dimension=0,
        tiled=True,
    )
    returned = lax.all_to_all(expert_out, "sp", split_axis=0, concat_axis=0, tiled=True)
    gathered_back = jnp.einsum("tks,sd->tkd", placing, returned, preferred_element_type=jnp.float32)
    weighted = jnp.sum(gathered_back * route_weight[:, :, None], axis=1)
    return (updated.astype(jnp.float32) + weighted).astype(jnp.bfloat16)


def solution(mesh):
    placed = (
        P(("grp", "sp", "tp"), None),
        P(("grp", "sp"), "tp"),
        P(("grp", "sp"), "tp"),
        P(("grp", "sp"), None),
        P(("grp", "sp"), None),
        P(),
        P(None, "tp"),
        P(None, "tp"),
        P("tp", None),
        P(),
        P(("grp", "sp", "tp"), None),
        P(("grp", "sp", "tp"), None),
        P(),
        P("sp", None, "tp"),
        P("sp", None, "tp"),
        P("sp", "tp", None),
    )
    return jax.shard_map(
        body, mesh=mesh, in_specs=placed, out_specs=P(("grp", "sp", "tp"), None), check_vma=False
    )
```

profile of v0, /device:TPU:0, one launch (start us, length us, event | category | flops | bytes accessed | tf_op | source)
XLA Modules:
  0.0 215.7 jit_solution(12267878147756269615)
XLA Ops:
  6.6 1.0 copy.40
  7.6 15.3 %all_gather.10 = bf16[1024,64]{0,1:T(8,128)(2,1)S(1)} all-gather(bf16[256,64]{0,1:T(8,128)(2,1)} %param.22), channel_id=1, replica_groups=mesh['grp'=2,'sp'=4,'tp'=4] {'sp'}, dimensions={0}, use_global_device_ids=true | all-gather | bytes 163840 | tf_op jit(solution)/shard_map/all_gather | solution.py:117
  22.9 16.2 %all_gather.9 = bf16[1024,256]{1,0:T(8,128)(2,1)S(1)} all-gather(bf16[256,256]{1,0:T(8,128)(2,1)} %param.21), channel_id=1, replica_groups=mesh['grp'=2,'sp'=4,'tp'=4] {'sp'}, dimensions={0}, use_global_device_ids=true | all-gather | bytes 655360 | tf_op jit(solution)/shard_map/all_gather | solution.py:116
  39.3 4.9 %conditional.1 = (f32[2,256]{1,0:T(2,128)S(1)}, f32[2,256,128]{1,2,0:T(8,128)S(1)}) conditional(s32[]{:T(128)} %convert_element_type.105, () %tuple.13, (s32[]{:T(128)}, s32[256]{0:T(256)S(1)}, bf16[1024,256]{1,0:T(8,128)(2,1)S(1)}, f32[256]{0:T(256)}, bf16[256,256]{1,0:T(8,128)(2,1)}, /*index=5*/bf16[256,256]{1,0:T(8,128)(2,1)}, ...), branch_computations={%region_0.0_spmd, %region_1.5_spmd} | conditional | flops 612468544 | bytes 17417576 | solution.py:129
  39.9 0.6 fusion.17
  40.4 1.4 convolution_convert_fusion
  41.9 0.5 convolution_convert_fusion.1
  42.4 0.5 fusion.20
  42.9 0.6 fusion.58
  43.4 0.5 fusion.7
  43.9 0.3 fusion.3
  44.3 1.5 convolution_convert_fusion.2
  46.9 24.3 %reduce-scatter.3.cloned.1.call-done = bf16[64,2048]{1,0:T(8,128)(2,1)} async-done(((bf16[256,2048]{1,0:T(8,128)(2,1)}), bf16[64,2048]{1,0:T(8,128)(2,1)}) %reduce-scatter.3.cloned.1.call-update) | async-done | bytes 262160 | tf_op jit(solution)/shard_map/reduce_scatter | solution.py:134
  71.2 1.1 fusion.40
  72.3 1.2 fusion.44
  73.6 0.4 convolution_convert_fusion.3
  74.0 24.4 %all_to_all.24 = bf16[4,48,2048]{2,1,0:T(8,128)(2,1)} all-to-all(bf16[4,48,2048]{2,1,0:T(8,128)(2,1)S(1)} %bitcast.63), channel_id=1, replica_groups=mesh['grp'=2,'sp'=4,'tp'=4] {'sp'}, dimensions={0} | all-to-all | bytes 1572864 | tf_op jit(solution)/shard_map/all_to_all | solution.py:158
  98.5 26.7 %all-gather.2.cloned.1.call-done = bf16[768,2048]{1,0:T(8,128)(2,1)} async-done(((bf16[192,2048]{1,0:T(8,128)(2,1)}), bf16[768,2048]{1,0:T(8,128)(2,1)}) %all-gather.2.cloned.1.call-update) | async-done | bytes 3145744 | tf_op jit(solution)/shard_map/all_gather | solution.py:159
  125.3 8.0 %fusion.28 = f32[768,896]{1,0:T(8,128)} fusion(bf16[768,2048]{1,0:T(8,128)(2,1)} %all-gather.2.cloned.1.call-done, bf16[1,2048,896]{2,1,0:T(8,128)(2,1)} %param.32), kind=kOutput, calls=%fused_computation.40 | convolution fusion | flops 2818572288 | bytes 9568256 | tf_op jit(solution)/shard_map/dot_general | solution.py:161
  133.3 12.2 %fusion.32 = bf16[768,2048]{1,0:T(8,128)(2,1)} fusion(bf16[1,896,2048]{2,1,0:T(8,128)(2,1)} %param.33, f32[768,896]{1,0:T(8,128)} %fusion.28, bf16[768,2048]{1,0:T(8,128)(2,1)} %all-gather.2.cloned.1.call-done, bf16[1,2048,896]{2,1,0:T(8,128)(2,1)} %param.31), kind=kOutput, calls=%fused_computation.44 | convolution fusion | flops 5642846208 | bytes 16384000 | tf_op jit(solution)/shard_map/dot_general | solution.py:164
  145.5 38.1 %reduce-scatter.5.cloned.1.call-done = bf16[192,2048]{1,0:T(8,128)(2,1)} async-done(((bf16[768,2048]{1,0:T(8,128)(2,1)}), bf16[192,2048]{1,0:T(8,128)(2,1)}) %reduce-scatter.5.cloned.1.call-update) | async-done | bytes 786448 | tf_op jit(solution)/shard_map/reduce_scatter | solution.py:165
  183.5 24.5 %all_to_all.25 = bf16[4,48,2048]{2,1,0:T(8,128)(2,1)S(1)} all-to-all(bf16[4,48,2048]{2,1,0:T(8,128)(2,1)} %bitcast.64), channel_id=1, replica_groups=mesh['grp'=2,'sp'=4,'tp'=4] {'sp'}, dimensions={0} | all-to-all | bytes 1572864 | tf_op jit(solution)/shard_map/all_to_all | solution.py:171
  208.1 0.4 fusion.37
  208.4 0.8 fusion.47
  (50 shorter events, 1.9 us)
Async XLA Ops:
  6.5 37.8 %copy-start = (bf16[256,2048]{1,0:T(8,128)(2,1)S(1)}, bf16[256,2048]{1,0:T(8,128)(2,1)}, u32[]{:S(2)}) copy-start(bf16[256,2048]{1,0:T(8,128)(2,1)} %param.26) | copy-start | bytes 3145732
  6.5 64.6 %reduce-scatter.3.cloned.1.call-start = ((), (), s32[]{:S(2)}) async-start(), calls=%async_computation.4 | async-start | bytes 1310720 | tf_op jit(solution)/shard_map/reduce_scatter | solution.py:134
  39.3 2.5 %copy-start.7 = (bf16[256,256]{1,0:T(8,128)(2,1)S(1)}, bf16[256,256]{1,0:T(8,128)(2,1)}, u32[]{:S(2)}) copy-start(bf16[256,256]{1,0:T(8,128)(2,1)} %get-tuple-element.44) | copy-start | bytes 393220 | tf_op jit(solution)/shard_map/cond
  39.4 2.5 %copy-start.8 = (f32[256]{0:T(256)S(1)}, f32[256]{0:T(256)}, u32[]{:S(2)}) copy-start(f32[256]{0:T(256)} %get-tuple-element.43) | copy-start | bytes 3076 | tf_op jit(solution)/shard_map/cond
  39.4 3.0 %copy-start.2 = (bf16[256,256]{1,0:T(8,128)(2,1)S(1)}, bf16[256,256]{1,0:T(8,128)(2,1)}, u32[]{:S(2)}) copy-start(bf16[256,256]{1,0:T(8,128)(2,1)} %get-tuple-element.45) | copy-start | bytes 393220 | tf_op jit(solution)/shard_map/cond
  44.2 1.6 copy-start.6
  44.2 28.0 %copy-start.1 = (bf16[64,2048]{1,0:T(8,128)(2,1)S(1)}, bf16[64,2048]{1,0:T(8,128)(2,1)}, u32[]{:S(2)}) copy-start(bf16[64,2048]{1,0:T(8,128)(2,1)} %param.18) | copy-start | bytes 786436
  44.2 28.0 %copy-start.3 = (f32[2048]{0:T(1024)S(1)}, f32[2048]{0:T(1024)}, u32[]{:S(2)}) copy-start(f32[2048]{0:T(1024)} %param.27) | copy-start | bytes 24580
  44.3 29.3 %copy-start.4 = (f32[2048]{0:T(1024)S(1)}, f32[2048]{0:T(1024)}, u32[]{:S(2)}) copy-start(f32[2048]{0:T(1024)} %param.30) | copy-start | bytes 24580
  45.8 79.5 %all-gather.2.cloned.1.call-start = ((), (), s32[]{:S(2)}) async-start(), calls=%async_computation.5 | async-start | bytes 3932160 | tf_op jit(solution)/shard_map/all_gather | solution.py:159
  98.5 85.1 %reduce-scatter.5.cloned.1.call-start = ((), (), s32[]{:S(2)}) async-start(), calls=%async_computation.6 | async-start | bytes 3932160 | tf_op jit(solution)/shard_map/reduce_scatter | solution.py:165
  145.4 62.6 %copy-start.5 = (f32[64,2]{0,1:T(2,128)S(1)}, f32[64,2]{0,1:T(2,128)}, u32[]{:S(2)}) copy-start(f32[64,2]{0,1:T(2,128)} %param.29) | copy-start | bytes 1540
Sparse Core Ops, SparseCore 0:
  45.9 25.1 reduce-scatter.2
  98.6 26.6 all-gather.1
  145.6 37.9 reduce-scatter.4
where the time goes:
time: 216 us
  waiting for transfers between devices  89.2 us (41%)
  blocking collectives  80.5 us (37%)
  matrix products  25.8 us (12%)
  between operations  13.3 us (6%)
  other arithmetic  5.23 us (2%)
    reduce_scatter x2, waiting for transfers between devices, body(): lax.psum_scatter(product.astype(jnp.bfloat16).astype(jnp.float32).astype(...  62.4 us
    all_gather x1, waiting for transfers between devices, body(): span_rows = lax.all_gather(received, 'tp', axis=0, tiled=True)  26.7 us
    all_to_all x1, blocking collectives, body(): lax.all_to_all(expert_out, 'sp', split_axis=0, concat_axis=0, tiled=True)  24.5 us
    all_to_all x1, blocking collectives, body(): lax.all_to_all(sending, 'sp', split_axis=0, concat_axis=0, tiled=True)  24.4 us
    all_gather x1, blocking collectives, body(): lax.all_gather(kv_latent, 'sp', axis=0, tiled=True)  16.2 us
    all_gather x1, blocking collectives, body(): lax.all_gather(rope_key, 'sp', axis=0, tiled=True)  15.3 us
    dot_general x1, matrix products, body(): product = jnp.dot(chosen, w_down[0], preferred_element_type=jnp.float32)  12.2 us
    dot_general x1, matrix products, body(): up_proj = jnp.dot(span_rows, w_up[0], preferred_element_type=jnp.float32)  8 us
  transfers between devices with their start and end apart: 3, of which 3 were waited for; matrix products, arithmetic and copies ran while one was open for 0% of the time, Pallas kernels for 0%

commit v1 on v0

--- a/solution.py
+++ b/solution.py
@@ -156,7 +156,12 @@
         jnp.bfloat16
     )
     received = lax.all_to_all(sending, "sp", split_axis=0, concat_axis=0, tiled=True)
-    span_rows = lax.all_gather(received, "tp", axis=0, tiled=True)
+    ring = [received]
+    for hop in range(3):
+        ring.append(lax.ppermute(ring[-1], "tp", [(dev, (dev + 1) % 4) for dev in range(4)]))
+    span_rows = jnp.roll(
+        jnp.concatenate(ring[::-1], axis=0), (lax.axis_index("tp") + 1) * ring[0].shape[0], axis=0
+    )
     gate_pre = jnp.dot(span_rows, w_gate[0], preferred_element_type=jnp.float32)
     up_proj = jnp.dot(span_rows, w_up[0], preferred_element_type=jnp.float32)
     hidden_rows = (jax.nn.silu(gate_pre) * up_proj).astype(jnp.bfloat16)

time: 216 us -> 225 us (1.042)
  local copies, waits for them, and re-layouts: 1.52 us -> 7.12 us
  waiting for transfers between devices: 89.2 us -> 94.8 us
    ppermute x0 -> x3, waiting for transfers between devices: none -> 34.3 us  [body(): lax.ppermute(ring[-1], 'tp', [(dev, (dev + 1) % 4) for dev in range(4)])]
    all_gather x1 -> x0, waiting for transfers between devices: 26.7 us -> none  [body(): span_rows = lax.all_gather(received, 'tp', axis=0, tiled=True)]
    unnamed x13 -> x28, local copies, waits for them, and re-layouts: 0.13 us -> 5.67 us
    dot_general x1, matrix products: 8 us -> 4.91 us  [body(): up_proj = jnp.dot(span_rows, w_up[0], preferred_element_type=jnp.float32)]
  transfers between devices with their start and end apart: 3 -> 5, of which waited for: 3 -> 5; matrix products, arithmetic and copies ran while one was open for 0% -> 0% of each run, Pallas kernels for 0% -> 0%
where the time goes in v1:
time: 225 us
  waiting for transfers between devices  94.8 us (42%)
  blocking collectives  80.4 us (36%)
  matrix products  23.8 us (11%)
  between operations  13.7 us (6%)
  local copies, waits for them, and re-layouts  7.12 us (3%)
  other arithmetic  5.22 us (2%)
    reduce_scatter x2, waiting for transfers between devices, body(): lax.psum_scatter(product.astype(jnp.bfloat16).astype(jnp.float32).astype(...  60.4 us
    ppermute x3, waiting for transfers between devices, body(): lax.ppermute(ring[-1], 'tp', [(dev, (dev + 1) % 4) for dev in range(4)])  34.3 us
    all_to_all x1, blocking collectives, body(): lax.all_to_all(expert_out, 'sp', split_axis=0, concat_axis=0, tiled=True)  24.5 us
    all_to_all x1, blocking collectives, body(): lax.all_to_all(sending, 'sp', split_axis=0, concat_axis=0, tiled=True)  24.3 us
    all_gather x1, blocking collectives, body(): lax.all_gather(kv_latent, 'sp', axis=0, tiled=True)  16.2 us
    all_gather x1, blocking collectives, body(): lax.all_gather(rope_key, 'sp', axis=0, tiled=True)  15.3 us
    dot_general x1, matrix products, body(): product = jnp.dot(chosen, w_down[0], preferred_element_type=jnp.float32)  12.2 us
    unnamed x28, local copies, waits for them, and re-layouts  5.67 us
  transfers between devices with their start and end apart: 5, of which 5 were waited for; matrix products, arithmetic and copies ran while one was open for 0% of the time, Pallas kernels for 0%

profile of v1, /device:TPU:0, one launch (start us, length us, event | category | flops | bytes accessed | tf_op | source)
XLA Modules:
  0.0 225.1 jit_solution(2556440639576791712)
XLA Ops:
  6.6 1.0 copy.40
  7.6 15.3 %all_gather.7 = bf16[1024,64]{0,1:T(8,128)(2,1)S(1)} all-gather(bf16[256,64]{0,1:T(8,128)(2,1)} %param.22), channel_id=1, replica_groups=mesh['grp'=2,'sp'=4,'tp'=4] {'sp'}, dimensions={0}, use_global_device_ids=true | all-gather | bytes 163840 | tf_op jit(solution)/shard_map/all_gather | solution.py:117
  22.9 16.2 %all_gather.6 = bf16[1024,256]{1,0:T(8,128)(2,1)S(1)} all-gather(bf16[256,256]{1,0:T(8,128)(2,1)} %param.21), channel_id=1, replica_groups=mesh['grp'=2,'sp'=4,'tp'=4] {'sp'}, dimensions={0}, use_global_device_ids=true | all-gather | bytes 655360 | tf_op jit(solution)/shard_map/all_gather | solution.py:116
  39.3 5.8 %conditional.1 = (f32[2,256]{1,0:T(2,128)S(1)}, f32[2,256,128]{1,2,0:T(8,128)S(1)}) conditional(s32[]{:T(128)} %convert_element_type.105, () %tuple.13, (s32[]{:T(128)}, s32[256]{0:T(256)S(1)}, bf16[1024,256]{1,0:T(8,128)(2,1)S(1)}, f32[256]{0:T(256)}, bf16[256,256]{1,0:T(8,128)(2,1)}, /*index=5*/bf16[256,256]{1,0:T(8,128)(2,1)}, ...), branch_computations={%region_0.0_spmd, %region_1.5_spmd} | conditional | flops 612468544 | bytes 16889136 | solution.py:129
  39.8 0.6 fusion.17
  40.4 1.4 convolution_convert_fusion
  41.8 1.4 convolution_convert_fusion.1
  43.7 0.6 fusion.68
  45.2 1.5 convolution_convert_fusion.2
  47.8 24.3 %reduce-scatter.3.cloned.1.call-done = bf16[64,2048]{1,0:T(8,128)(2,1)} async-done(((bf16[256,2048]{1,0:T(8,128)(2,1)}), bf16[64,2048]{1,0:T(8,128)(2,1)}) %reduce-scatter.3.cloned.1.call-update) | async-done | bytes 262160 | tf_op jit(solution)/shard_map/reduce_scatter | solution.py:134
  72.0 1.1 fusion.47
  73.2 1.2 fusion.51
  74.9 24.3 %all_to_all.24 = bf16[4,48,2048]{2,1,0:T(8,128)(2,1)S(1)} all-to-all(bf16[4,48,2048]{2,1,0:T(8,128)(2,1)S(1)} %bitcast.63), channel_id=1, replica_groups=mesh['grp'=2,'sp'=4,'tp'=4] {'sp'}, dimensions={0} | all-to-all | bytes 1572864 | tf_op jit(solution)/shard_map/all_to_all | solution.py:158
  99.2 11.4 %collective-permute-done = bf16[192,2048]{1,0:T(8,128)(2,1)S(1)} collective-permute-done((bf16[192,2048]{1,0:T(8,128)(2,1)S(1)}, bf16[192,2048]{1,0:T(8,128)(2,1)S(1)}, u32[]{:S(2)}, u32[]{:S(2)}) %collective-permute-start) | collective-permute-done | bytes 786464 | tf_op jit(solution)/shard_map/ppermute | solution.py:161
  110.6 11.4 %collective-permute-done.1 = bf16[192,2048]{1,0:T(8,128)(2,1)S(1)} collective-permute-done((bf16[192,2048]{1,0:T(8,128)(2,1)S(1)}, bf16[192,2048]{1,0:T(8,128)(2,1)S(1)}, u32[]{:S(2)}, u32[]{:S(2)}) %collective-permute-start.1) | collective-permute-done | bytes 786464 | tf_op jit(solution)/shard_map/ppermute | solution.py:161
  122.0 11.5 %collective-permute-done.2 = bf16[192,2048]{1,0:T(8,128)(2,1)} collective-permute-done((bf16[192,2048]{1,0:T(8,128)(2,1)S(1)}, bf16[192,2048]{1,0:T(8,128)(2,1)}, u32[]{:S(2)}, u32[]{:S(2)}) %collective-permute-start.2) | collective-permute-done | bytes 786464 | tf_op jit(solution)/shard_map/ppermute | solution.py:161
  133.6 1.2 constant_dynamic-update-slice_fusion.7
  135.0 1.3 constant_dynamic-update-slice_fusion.3
  136.6 2.7 %copy-done.5 = bf16[1536,2048]{1,0:T(8,128)(2,1)} copy-done((bf16[1536,2048]{1,0:T(8,128)(2,1)}, bf16[1536,2048]{1,0:T(8,128)(2,1)S(1)}, u32[]{:S(2)}) %copy-start.5) | copy-done | bytes 6291480
  139.2 4.9 %fusion.28 = f32[768,896]{1,0:T(8,128)} fusion(bf16[1,2048,896]{2,1,0:T(8,128)(2,1)S(1)} %copy-done.10, bf16[1536,2048]{1,0:T(8,128)(2,1)S(1)} %constant_dynamic-update-slice_fusion, s32[]{:T(128)S(6)} %select_n.18), kind=kOutput, calls=%fused_computation.40 | convolution fusion | flops 2818572288 | bytes 9568260 | tf_op jit(solution)/shard_map/dot_general | solution.py:166
  144.1 12.2 %fusion.32 = bf16[768,2048]{1,0:T(8,128)(2,1)} fusion(bf16[1,896,2048]{2,1,0:T(8,128)(2,1)} %param.33, f32[768,896]{1,0:T(8,128)} %fusion.28, bf16[1,2048,896]{2,1,0:T(8,128)(2,1)} %param.31, bf16[1536,2048]{1,0:T(8,128)(2,1)} %copy-done.5, s32[]{:T(128)S(6)} %select_n.18), kind=kOutput, calls=%fused_computation.44 | convolution fusion | flops 5642846208 | bytes 16384004 | tf_op jit(solution)/shard_map/dot_general | solution.py:169
  156.4 36.2 %reduce-scatter.5.cloned.1.call-done = bf16[192,2048]{1,0:T(8,128)(2,1)} async-done(((bf16[768,2048]{1,0:T(8,128)(2,1)}), bf16[192,2048]{1,0:T(8,128)(2,1)}) %reduce-scatter.5.cloned.1.call-update) | async-done | bytes 786448 | tf_op jit(solution)/shard_map/reduce_scatter | solution.py:170
  192.6 24.5 %all_to_all.25 = bf16[4,48,2048]{2,1,0:T(8,128)(2,1)S(1)} all-to-all(bf16[4,48,2048]{2,1,0:T(8,128)(2,1)} %bitcast.64), channel_id=1, replica_groups=mesh['grp'=2,'sp'=4,'tp'=4] {'sp'}, dimensions={0} | all-to-all | bytes 1572864 | tf_op jit(solution)/shard_map/all_to_all | solution.py:176
  217.5 0.8 fusion.54
  (65 shorter events, 4.3 us)
Async XLA Ops:
  6.5 38.7 %copy-start = (bf16[256,2048]{1,0:T(8,128)(2,1)S(1)}, bf16[256,2048]{1,0:T(8,128)(2,1)}, u32[]{:S(2)}) copy-start(bf16[256,2048]{1,0:T(8,128)(2,1)} %param.26) | copy-start | bytes 3145732
  6.5 65.5 %reduce-scatter.3.cloned.1.call-start = ((), (), s32[]{:S(2)}) async-start(), calls=%async_computation.4 | async-start | bytes 1310720 | tf_op jit(solution)/shard_map/reduce_scatter | solution.py:134
  39.3 3.9 %copy-start.4 = (bf16[256,256]{1,0:T(8,128)(2,1)S(1)}, bf16[256,256]{1,0:T(8,128)(2,1)}, u32[]{:S(2)}) copy-start(bf16[256,256]{1,0:T(8,128)(2,1)} %get-tuple-element.45) | copy-start | bytes 393220 | tf_op jit(solution)/shard_map/cond
  45.1 1.6 copy-start.9
  45.1 28.0 %copy-start.3 = (bf16[64,2048]{1,0:T(8,128)(2,1)S(1)}, bf16[64,2048]{1,0:T(8,128)(2,1)}, u32[]{:S(2)}) copy-start(bf16[64,2048]{1,0:T(8,128)(2,1)} %param.18) | copy-start | bytes 786436
  45.1 28.0 %copy-start.6 = (f32[2048]{0:T(1024)S(1)}, f32[2048]{0:T(1024)}, u32[]{:S(2)}) copy-start(f32[2048]{0:T(1024)} %param.27) | copy-start | bytes 24580
  45.1 29.3 %copy-start.7 = (f32[2048]{0:T(1024)S(1)}, f32[2048]{0:T(1024)}, u32[]{:S(2)}) copy-start(f32[2048]{0:T(1024)} %param.30) | copy-start | bytes 24580
  46.7 145.9 %reduce-scatter.5.cloned.1.call-start = ((), (), s32[]{:S(2)}) async-start(), calls=%async_computation.5 | async-start | bytes 3932160 | tf_op jit(solution)/shard_map/reduce_scatter | solution.py:170
  74.4 47.6 %copy-start.1 = (bf16[64,2048]{1,0:T(8,128)(2,1)}, bf16[64,2048]{1,0:T(8,128)(2,1)S(1)}, u32[]{:S(2)}) copy-start(bf16[64,2048]{1,0:T(8,128)(2,1)S(1)} %get-tuple-element.49) | copy-start | bytes 786436
  99.2 11.4 %collective-permute-start = (bf16[192,2048]{1,0:T(8,128)(2,1)S(1)}, bf16[192,2048]{1,0:T(8,128)(2,1)S(1)}, u32[]{:S(2)}, u32[]{:S(2)}) collective-permute-start(bf16[192,2048]{1,0:T(8,128)(2,1)S(1)} %bitcast.59), channel_id=1, source_target_pairs={{0,1},{1,2},{2,3},{3,0},{4,5},{5,6},{6,7},{7,4},{8,9},{9,10},{10,1... | collective-permute-start | bytes 2359304 | tf_op jit(solution)/shard_map/ppermute | solution.py:161
  110.6 11.4 %collective-permute-start.1 = (bf16[192,2048]{1,0:T(8,128)(2,1)S(1)}, bf16[192,2048]{1,0:T(8,128)(2,1)S(1)}, u32[]{:S(2)}, u32[]{:S(2)}) collective-permute-start(bf16[192,2048]{1,0:T(8,128)(2,1)S(1)} %collective-permute-done), channel_id=1, source_target_pairs={{0,1},{1,2},{2,3},{3,0},{4,5},{5,6},{6,7},{7,4},{8,9},{9,10},{10,1... | collective-permute-start | bytes 2359304 | tf_op jit(solution)/shard_map/ppermute | solution.py:161
  122.0 11.5 %collective-permute-start.2 = (bf16[192,2048]{1,0:T(8,128)(2,1)S(1)}, bf16[192,2048]{1,0:T(8,128)(2,1)}, u32[]{:S(2)}, u32[]{:S(2)}) collective-permute-start(bf16[192,2048]{1,0:T(8,128)(2,1)S(1)} %collective-permute-done.1), channel_id=1, source_target_pairs={{0,1},{1,2},{2,3},{3,0},{4,5},{5,6},{6,7},{7,4},{8,9},{9,10},{10,1... | collective-permute-start | bytes 2359304 | tf_op jit(solution)/shard_map/ppermute | solution.py:161
  134.9 4.3 %copy-start.10 = (bf16[1,2048,896]{2,1,0:T(8,128)(2,1)S(1)}, bf16[1,2048,896]{2,1,0:T(8,128)(2,1)}, u32[]{:S(2)}) copy-start(bf16[1,2048,896]{2,1,0:T(8,128)(2,1)} %param.32) | copy-start | bytes 11010052
  136.6 2.7 %copy-start.5 = (bf16[1536,2048]{1,0:T(8,128)(2,1)}, bf16[1536,2048]{1,0:T(8,128)(2,1)S(1)}, u32[]{:S(2)}) copy-start(bf16[1536,2048]{1,0:T(8,128)(2,1)S(1)} %constant_dynamic-update-slice_fusion) | copy-start | bytes 18874372
  156.4 60.7 %copy-start.8 = (f32[64,2]{0,1:T(2,128)S(1)}, f32[64,2]{0,1:T(2,128)}, u32[]{:S(2)}) copy-start(f32[64,2]{0,1:T(2,128)} %param.29) | copy-start | bytes 1540
  156.4 61.1 %copy-start.2 = (bf16[64,2048]{1,0:T(8,128)(2,1)S(1)}, bf16[64,2048]{1,0:T(8,128)(2,1)}, u32[]{:S(2)}) copy-start(bf16[64,2048]{1,0:T(8,128)(2,1)} %copy-done.1) | copy-start | bytes 786436
Sparse Core Ops, SparseCore 0:
  46.8 25.1 reduce-scatter.2
  156.5 35.9 reduce-scatter.4
